TPU v7x, 256 devices: a whole 4x4x8 slice. The times are simulated.
256 devices in a mesh: ep: 64 (over z, y, x_hi), tp: 4 (over x_lo, core).
Axes of the slice: x: 4 (x_hi: 2, x_lo: 2; x = x_hi * 2 + x_lo), y: 4, z: 8, core: 2. Of those that a mesh axis runs over, the one named last changes fastest.
Arguments:
- tokens: bfloat16 [1536, 1024], P('ep'), may hold values from -3 to 3
- attn_gain: float32 [1024], replicated, may hold values from 0.1 to 1.9
- w_query: bfloat16 [1024, 1024], P(None, 'tp'), may hold values from -0.1875 to 0.1875
- w_key: bfloat16 [1024, 256], P(None, 'tp'), may hold values from -0.1875 to 0.1875
- w_value: bfloat16 [1024, 256], P(None, 'tp'), may hold values from -0.1875 to 0.1875
- attn_bias: float32 [16], P('tp'), may hold values from -7.5 to -3
- key_cache: bfloat16 [1536, 256, 1024], P('ep', 'tp'), may hold values from -6 to 6
- value_cache: bfloat16 [1536, 256, 1024], P('ep', 'tp'), may hold values from -6 to 6
- lengths: int32 [1536], P('ep'), may hold values from 128 to 1024
- w_out: bfloat16 [1024, 1024], P('tp'), may hold values from -0.75 to 0.75
- ffn_gain: float32 [1024], replicated, may hold values from 0.1 to 1.9
- routes: int32 [1536, 2], P('ep'), may hold values from 0 to 63, all different within a row; in each aligned block of 24 rows (0 to 23, 24 to 47, ...) at most 2 rows name the same one
- route_weight: float32 [1536, 2], P('ep'), may hold values from 0.2 to 1
- expert_gate: bfloat16 [64, 1024, 3584], P('ep', None, 'tp'), may hold values from -0.1875 to 0.1875
- expert_up: bfloat16 [64, 1024, 3584], P('ep', None, 'tp'), may hold values from -0.1875 to 0.1875
- expert_down: bfloat16 [64, 3584, 1024], P('ep', 'tp'), may hold values from -0.09375 to 0.09375
Outputs:
- mixed: bfloat16 [1536, 1024], P('ep')
- new_keys: bfloat16 [1536, 256], P('ep', 'tp')
- new_values: bfloat16 [1536, 256], P('ep', 'tp')
Inputs may be any that keep to these rules, and one draw needn't show every extreme that they name: `routes`: each row names 2 different experts. Among the rows of one device no expert is named by more than 2 of them, and on some device some expert is named by exactly 2.
All inputs are finite; a program needn't handle non-finite values.
Results may differ from a plain program's by a relative error of at most 0.02.
Values may be sent and summed in bfloat16 or wider, within the bound.
A program may use at most 64 MiB of HBM per device.

v0:
```python
import math

import jax
import jax.numpy as jnp
from jax import lax
from jax.sharding import PartitionSpec as P

HEADS = 16
KV_HEADS = 4
HEAD = 64


norm_epsilon = 1e-06


def total_of_pieces(array, axis):
    return lax.all_gather(array, axis).astype(jnp.float32).sum(0)


def split_up(array, dim, devices):
    before, after = (array.shape[:dim], array.shape[dim + 1 :])
    return jnp.moveaxis(array.reshape(*before, devices, -1, *after), dim, 0)


def sum_at_owner(array, axis, dim):
    tiles = split_up(array, dim, lax.axis_size(axis))
    arrived = lax.all_to_all(tiles, axis, split_axis=0, concat_axis=0, tiled=True)
    return arrived.astype(jnp.float32).sum(axis=0)


def joined_along(tiles, dim):
    tiles = jnp.moveaxis(tiles, 0, dim)
    shape = tiles.shape
    return tiles.reshape(*shape[:dim], shape[dim] * shape[dim + 1], *shape[dim + 2 :])


def copy_for_each(array, axis):
    copies = jnp.broadcast_to(array, (lax.axis_size(axis), *array.shape))
    return lax.all_to_all(copies, axis, split_axis=0, concat_axis=0, tiled=True)


def collect(array, axis, dim):
    return joined_along(copy_for_each(array, axis), dim)


def rms_scale(inputs, gains):
    widened = inputs.astype(jnp.float32)
    factor = lax.rsqrt(jnp.mean(widened * widened, axis=-1, keepdims=True) + norm_epsilon)
    return (widened * factor * gains).astype(jnp.bfloat16)


def dispatch_matrix(block_routes, experts, capacity):
    flat_routes = block_routes.reshape(-1)
    onehot = (flat_routes[:, None] == jnp.arange(experts, dtype=jnp.int32)[None, :]).astype(
        jnp.float32
    )
    row_total = flat_routes.shape[0]
    row_ids = jnp.arange(row_total, dtype=jnp.int32)
    earlier = (row_ids[None, :] < row_ids[:, None]).astype(jnp.float32)
    before = jnp.dot(earlier, onehot)
    slot_index = jnp.sum(before * onehot, axis=1).astype(jnp.int32)
    target = flat_routes * capacity + slot_index
    return jnp.arange(experts * capacity, dtype=jnp.int32)[:, None] == target[None, :]


def suffix_totals(log_fall):
    lead_shape = log_fall.shape[:-1]
    key_span = log_fall.shape[-1]
    block_len = math.gcd(key_span, 128)
    block_count = key_span // block_len
    blocked = log_fall.reshape(lead_shape + (block_count, block_len))
    inner_ids = jnp.arange(block_len, dtype=jnp.int32)
    upper_mask = (inner_ids[:, None] >= inner_ids[None, :]).astype(jnp.float32)
    within = jnp.einsum("...bj,ji->...bi", blocked, upper_mask)
    block_sums = jnp.sum(blocked, axis=-1)
    block_ids = jnp.arange(block_count, dtype=jnp.int32)
    later_mask = (block_ids[:, None] > block_ids[None, :]).astype(jnp.float32)
    later = jnp.einsum("...c,cb->...b", block_sums, later_mask)
    return (within + later[..., None]).reshape(lead_shape + (key_span,))


def stick_read(queries, key_block, value_block, bias_grid, lengths):
    row_count, kv_count, group_size, head_size = queries.shape
    key_span = key_block.shape[2]
    key_heads = key_block.reshape(row_count, kv_count, head_size, key_span)
    value_heads = value_block.reshape(row_count, kv_count, head_size, key_span)
    scores = jnp.einsum("skgd,skdl->skgl", queries, key_heads, preferred_element_type=jnp.float32)
    scores = scores * head_size ** (-0.5) + bias_grid[None, :, :, None]
    inside = (jnp.arange(key_span, dtype=jnp.int32)[None, :] < lengths[:, None])[:, None, None, :]
    log_fall = jnp.where(inside, jax.nn.log_sigmoid(-scores), 0.0)
    log_after = suffix_totals(log_fall) - log_fall
    weights = jnp.where(inside, jnp.exp(jax.nn.log_sigmoid(scores) + log_after), 0.0).astype(
        jnp.bfloat16
    )
    mixed_out = jnp.einsum(
        "skgl,skdl->skgd", weights, value_heads, preferred_element_type=jnp.float32
    )
    return mixed_out.astype(jnp.bfloat16).reshape(row_count, -1)


def body(
    tokens,
    attn_gain,
    w_query,
    w_key,
    w_value,
    attn_bias,
    key_cache,
    value_cache,
    lengths,
    w_out,
    ffn_gain,
    routes,
    route_weight,
    expert_gate,
    expert_up,
    expert_down,
):
    seq_count, model_width = tokens.shape
    normed = rms_scale(tokens, attn_gain)
    queries = jnp.dot(normed, w_query, preferred_element_type=jnp.float32).astype(jnp.bfloat16)
    new_keys = jnp.dot(normed, w_key, preferred_element_type=jnp.float32).astype(jnp.bfloat16)
    new_values = jnp.dot(normed, w_value, preferred_element_type=jnp.float32).astype(jnp.bfloat16)
    kv_local = w_key.shape[1] // HEAD
    group_size = HEADS // KV_HEADS
    grouped = queries.reshape(seq_count, kv_local, group_size, HEAD)
    bias_grid = attn_bias.reshape(kv_local, group_size)
    attended = stick_read(grouped, key_cache, value_cache, bias_grid, lengths)
    partial_out = jnp.dot(attended, w_out, preferred_element_type=jnp.float32)
    attn_total = total_of_pieces(partial_out.astype(jnp.bfloat16), "tp").astype(jnp.float32)
    residual = (tokens.astype(jnp.float32) + attn_total).astype(jnp.bfloat16)
    normed_two = rms_scale(residual, ffn_gain)
    expert_count = lax.axis_size("ep")
    top_count = routes.shape[1]
    capacity = max(2, 2 * seq_count * top_count // expert_count)
    route_plan = dispatch_matrix(routes, expert_count, capacity).astype(jnp.bfloat16)
    repeated = jnp.repeat(normed_two, top_count, axis=0)
    outgoing = jnp.dot(route_plan, repeated, preferred_element_type=jnp.float32).astype(
        jnp.bfloat16
    )
    outgoing = outgoing.reshape(expert_count, capacity, model_width)
    gate_local = expert_gate[0]
    up_local = expert_up[0]
    down_local = expert_down[0]
    arrived = lax.all_to_all(outgoing, "ep", split_axis=0, concat_axis=0, tiled=True)
    sources, slot_count, row_width = arrived.shape
    row_block = arrived.reshape(sources * slot_count, row_width)
    gate_act = jnp.dot(row_block, gate_local, preferred_element_type=jnp.float32)
    lifted = jnp.dot(row_block, up_local, preferred_element_type=jnp.float32)
    hidden = (jax.nn.silu(gate_act) * lifted).astype(jnp.bfloat16)
    partial_value = jnp.dot(hidden, down_local, preferred_element_type=jnp.float32)
    share_part = sum_at_owner(partial_value.astype(jnp.bfloat16), "tp", 1).astype(jnp.bfloat16)
    returned = lax.all_to_all(
        share_part.reshape(sources, slot_count, -1), "ep", split_axis=0, concat_axis=0, tiled=True
    )
    flat_back = returned.reshape(expert_count * capacity, -1)
    picked = jnp.dot(route_plan.T, flat_back, preferred_element_type=jnp.float32)
    picked = picked.reshape(seq_count, top_count, -1)
    moe_sum = jnp.sum(picked * route_weight[:, :, None], axis=1)
    share_width = model_width // lax.axis_size("tp")
    own_cols = lax.dynamic_slice_in_dim(
        residual, lax.axis_index("tp") * share_width, share_width, 1
    )
    mixed_share = (own_cols.astype(jnp.float32) + moe_sum).astype(jnp.bfloat16)
    mixed_rows = collect(mixed_share, "tp", 1)
    return (mixed_rows, new_keys, new_values)


def solution(mesh):
    return jax.shard_map(
        body,
        mesh=mesh,
        in_specs=(
            P("ep", None),
            P(),
            P(None, "tp"),
            P(None, "tp"),
            P(None, "tp"),
            P("tp"),
            P("ep", "tp", None),
            P("ep", "tp", None),
            P("ep"),
            P("tp", None),
            P(),
            P("ep", None),
            P("ep", None),
            P("ep", None, "tp"),
            P("ep", None, "tp"),
            P("ep", "tp", None),
        ),
        out_specs=(P("ep", None), P("ep", "tp"), P("ep", "tp")),
        check_vma=False,
    )
```

profile of v0, /device:TPU:1, one launch (start us, length us, event | category | flops | bytes accessed | tf_op | source)
XLA Modules:
  0.0 103.6 jit_solution(11322441114298651713)
XLA Ops:
  0.6 0.0 copy-start
  0.6 1.1 %fusion.39 = f32[24]{0:T(128)S(1)} fusion(bf16[24,1024]{1,0:T(8,128)(2,1)} %param.16), kind=kLoop, calls=%fused_computation.49 | loop fusion | flops 73704 | bytes 49248 | tf_op jit(solution)/shard_map/reduce_sum | solution.py:48
  1.7 0.0 copy-start.9
  1.7 0.5 copy-done.9
  2.2 1.3 %convolution_convert_fusion.3 = bf16[24,256]{1,0:T(8,128)(2,1)S(1)} fusion(bf16[1024,256]{1,0:T(8,128)(2,1)} %param.18, bf16[24,1024]{1,0:T(8,128)(2,1)} %param.16, f32[1024]{0:T(1024)} %param.17, f32[24]{0:T(128)S(1)} %add_rsqrt_fusion.1), kind=kOutput, calls=%fused_computation.20 | convolution fusion | flops 12687360 | bytes 589920 | tf_op jit(solution)/shard_map/dot_general | solution.py:121
  3.6 0.1 reshape.176
  3.6 0.7 iota_compare_fusion
  4.4 0.0 copy-done
  4.4 0.0 copy-start.3
  4.4 2.4 %fusion.31 = (f32[24,4,1024]{2,1,0:T(4,128)}, f32[24,4,1024]{2,1,0:T(4,128)}) fusion(pred[24,1024]{1,0:T(8,128)(4,1)S(1)} %iota_compare_fusion, f32[4]{0:T(128)} %param.21, bf16[24,4,64]{2,1,0:T(4,128)(2,1)S(1)} %reshape.176, bf16[24,64,1024]{2,1,0:T(8,128)(2,1)S(1)} %copy-done), kind=kOutput, calls=%fused_computation.35 | convolution fusion | flops 13565952 | bytes 3969040 | tf_op jit(solution)/shard_map/skgd,skdl->skgl/dot_general | solution.py:87
  6.8 0.0 copy-done.3
  6.8 1.2 %reshape.177 = f32[24,4,8,128]{3,2,1,0:T(8,128)S(1)} reshape(f32[24,4,1024]{2,1,0:T(4,128)} %get-tuple-element.5) | data formatting | bytes 786432 | tf_op jit(solution)/shard_map/reshape.6
  7.9 0.8 reduce_sum.67
  8.8 0.9 fusion.45
  9.6 0.7 copy.30
  10.4 1.7 %convolution_add_fusion = f32[24,4,8,128]{3,2,1,0:T(8,128)} fusion(f32[24,4,8,128]{3,2,1,0:T(8,128)S(1)} %reshape.177, f32[24,4,8]{2,1,0:T(4,128)} %copy.30), kind=kOutput, calls=%fused_computation.9 | convolution fusion | flops 25280512 | bytes 789504 | tf_op jit(solution)/shard_map/...bj,ji->...bi/dot_general | solution.py:74
  12.1 1.9 %reshape.178 = f32[24,4,1024]{2,1,0:T(4,128)} reshape(f32[24,4,8,128]{3,2,1,0:T(8,128)} %convolution_add_fusion) | data formatting | bytes 786432 | tf_op jit(solution)/shard_map/reshape | solution.py:79
  14.0 0.0 copy-start.1
  14.0 0.0 copy-start.5
  14.0 0.0 copy-start.8
  14.0 3.5 %convolution_convert_fusion.2 = bf16[24,4,64]{2,1,0:T(4,128)(2,1)S(1)} fusion(bf16[24,64,1024]{2,1,0:T(8,128)(2,1)} %param.23, f32[24,4,1024]{2,1,0:T(4,128)} %reshape.178, f32[24,4,1024]{2,1,0:T(4,128)} %get-tuple-element.6, pred[24,1024]{1,0:T(8,128)(4,1)} %copy-done.3), kind=kOutput, calls=%fused_computation.17 | convolution fusion | flops 14555136 | bytes 3969024 | tf_op jit(solution)/shard_map/skgl,skdl->skgd/dot_general | solution.py:95
  17.5 0.1 reshape.179
  17.6 1.2 %convolution_convert_fusion.1 = bf16[24,1024]{1,0:T(8,128)(2,1)S(1)} fusion(bf16[24,256]{1,0:T(8,128)(2,1)S(1)} %reshape.179, bf16[256,1024]{1,0:T(8,128)(2,1)} %param.25), kind=kOutput, calls=%fused_computation.15 | convolution fusion | flops 12607488 | bytes 585728 | tf_op jit(solution)/shard_map/dot_general | solution.py:129
  18.8 8.6 %all-gather = bf16[96,1024]{1,0:T(8,128)(2,1)S(1)} all-gather(bf16[24,1024]{1,0:T(8,128)(2,1)S(1)} %convolution_convert_fusion.1), channel_id=2, replica_groups=mesh['ep'=64,'tp'=4] {'tp'}, dimensions={0}, use_global_device_ids=true | all-gather | bytes 245760 | tf_op jit(solution)/shard_map/all_gather | solution.py:17
  27.4 0.0 copy-done.1
  27.5 0.1 fusion.36
  27.6 0.0 copy-start.2
  27.6 0.6 copy-done.2
  28.2 0.0 copy-done.5
  28.2 0.1 fusion.38
  28.3 0.1 broadcast_in_dim.19
  28.4 0.0 copy-done.8
  28.4 0.1 copy.31
  28.5 0.1 reshape.180
  28.6 0.3 fusion.19
  28.9 0.0 copy-start.6
  28.9 0.5 copy-done.6
  29.4 0.2 convolution_convert_fusion
  29.6 0.8 reshape.182
  30.4 12.8 %all-to-all-start = ((bf16[64,2,1024]{2,1,0:T(2,128)(2,1)}), bf16[64,2,1024]{2,1,0:T(2,128)(2,1)}, u32[]{:S(2)}, u32[]{:S(2)}) async-start(bf16[64,2,1024]{2,1,0:T(2,128)(2,1)} %reshape.182), calls=%async_computation | async-start | bytes 524288 | tf_op jit(solution)/shard_map/all_to_all | solution.py:145
  43.3 12.7 %all-to-all-done = bf16[64,2,1024]{2,1,0:T(2,128)(2,1)} async-done(((bf16[64,2,1024]{2,1,0:T(2,128)(2,1)}), bf16[64,2,1024]{2,1,0:T(2,128)(2,1)}, u32[]{:S(2)}, u32[]{:S(2)}) %all-to-all-start) | async-done | bytes 262176 | tf_op jit(solution)/shard_map/all_to_all | solution.py:145
  56.0 1.0 %reshape.183 = bf16[128,1024]{1,0:T(8,128)(2,1)S(1)} reshape(bf16[64,2,1024]{2,1,0:T(2,128)(2,1)} %all-to-all-done) | data formatting | bytes 524288 | tf_op jit(solution)/shard_map/reshape | solution.py:147
  57.0 2.7 %fusion.4 = f32[128,896]{1,0:T(8,128)} fusion(bf16[128,1024]{1,0:T(8,128)(2,1)S(1)} %reshape.183, bf16[1,1024,896]{2,1,0:T(8,128)(2,1)} %param.29), kind=kOutput, calls=%fused_computation.4 | convolution fusion | flops 234881024 | bytes 2555904 | tf_op jit(solution)/shard_map/dot_general | solution.py:148
  59.7 0.0 copy-start.7
  59.7 3.7 %fusion.9 = bf16[128,1024]{1,0:T(8,128)(2,1)} fusion(bf16[1,896,1024]{2,1,0:T(8,128)(2,1)} %param.31, bf16[128,1024]{1,0:T(8,128)(2,1)S(1)} %reshape.183, bf16[1,1024,896]{2,1,0:T(8,128)(2,1)} %param.30, f32[128,896]{1,0:T(8,128)} %fusion.4), kind=kOutput, calls=%fused_computation.7 | convolution fusion | flops 470581248 | bytes 4653056 | tf_op jit(solution)/shard_map/dot_general | solution.py:151
  63.5 1.7 %copy.43 = bf16[16,4,8,256]{3,2,0,1:T(8,128)(2,1)} copy(bf16[16,4,8,256]{3,2,1,0:T(8,128)(2,1)} %bitcast.54) | data formatting | bytes 524288 | tf_op jit(solution)/shard_map/reshape | solution.py:22
  65.1 5.6 %all-to-all-start.1 = ((bf16[4,128,256]{2,1,0:T(8,128)(2,1)}), bf16[4,128,256]{2,1,0:T(8,128)(2,1)S(1)}, u32[]{:S(2)}, u32[]{:S(2)}) async-start(bf16[4,128,256]{2,1,0:T(8,128)(2,1)} %bitcast.52), calls=%async_computation.1 | async-start | bytes 524288 | tf_op jit(solution)/shard_map/all_to_all | solution.py:27
  70.7 0.0 copy-done.7
  70.7 0.1 iota_compare_fusion.6
  70.8 4.9 %all-to-all-done.1 = bf16[4,128,256]{2,1,0:T(8,128)(2,1)S(1)} async-done(((bf16[4,128,256]{2,1,0:T(8,128)(2,1)}), bf16[4,128,256]{2,1,0:T(8,128)(2,1)S(1)}, u32[]{:S(2)}, u32[]{:S(2)}) %all-to-all-start.1) | async-done | bytes 262176 | tf_op jit(solution)/shard_map/all_to_all | solution.py:27
  75.8 0.6 reshape.185
  76.5 5.0 %all-to-all-start.2 = ((bf16[64,2,256]{2,1,0:T(2,128)(2,1)}), bf16[64,2,256]{2,1,0:T(2,128)(2,1)S(1)}, u32[]{:S(2)}, u32[]{:S(2)}) async-start(bf16[64,2,256]{2,1,0:T(2,128)(2,1)} %reshape.185), calls=%async_computation.2 | async-start | bytes 131072 | tf_op jit(solution)/shard_map/all_to_all | solution.py:153
  81.5 0.0 copy-done.4
  81.5 0.0 copy-done.10
  81.5 1.7 %convolution_convert_fusion.4 = bf16[24,64]{1,0:T(8,128)(2,1)} fusion(bf16[1024,64]{0,1:T(8,128)(2,1)} %param.20, bf16[24,1024]{1,0:T(8,128)(2,1)S(1)} %copy-done.1, f32[1024]{0:T(1024)S(1)} %copy-done.4, f32[24]{0:T(128)S(1)} %copy-done.10), kind=kOutput, calls=%fused_computation.22 | convolution fusion | flops 3245568 | bytes 187488 | tf_op jit(solution)/shard_map/dot_general | solution.py:123
  83.2 9.3 %all-to-all-done.2 = bf16[64,2,256]{2,1,0:T(2,128)(2,1)S(1)} async-done(((bf16[64,2,256]{2,1,0:T(2,128)(2,1)}), bf16[64,2,256]{2,1,0:T(2,128)(2,1)S(1)}, u32[]{:S(2)}, u32[]{:S(2)}) %all-to-all-start.2) | async-done | bytes 65568 | tf_op jit(solution)/shard_map/all_to_all | solution.py:153
  92.6 0.0 copy-done.11
  92.6 0.1 fusion.18
  92.7 0.8 add_convert_fusion
  93.5 0.6 broadcast_in_dim.20
  94.1 5.6 %all-to-all-start.3 = ((bf16[4,24,256]{2,1,0:T(8,128)(2,1)}), bf16[4,24,256]{2,1,0:T(8,128)(2,1)S(1)}, u32[]{:S(2)}, u32[]{:S(2)}) async-start(bf16[4,24,256]{2,1,0:T(8,128)(2,1)} %broadcast_in_dim.20), calls=%async_computation.3 | async-start | bytes 98304 | tf_op jit(solution)/shard_map/all_to_all | solution.py:39
  99.7 1.7 %convolution_convert_fusion.5 = bf16[24,64]{1,0:T(8,128)(2,1)} fusion(bf16[1024,64]{0,1:T(8,128)(2,1)} %param.19, bf16[24,1024]{1,0:T(8,128)(2,1)S(1)} %copy-done.1, f32[1024]{0:T(1024)S(1)} %copy-done.4, f32[24]{0:T(128)S(1)} %copy-done.10), kind=kOutput, calls=%fused_computation.23 | convolution fusion | flops 3245568 | bytes 187488 | tf_op jit(solution)/shard_map/dot_general | solution.py:122
  101.4 1.5 %all-to-all-done.3 = bf16[4,24,256]{2,1,0:T(8,128)(2,1)S(1)} async-done(((bf16[4,24,256]{2,1,0:T(8,128)(2,1)}), bf16[4,24,256]{2,1,0:T(8,128)(2,1)S(1)}, u32[]{:S(2)}, u32[]{:S(2)}) %all-to-all-start.3) | async-done | bytes 49184 | tf_op jit(solution)/shard_map/all_to_all | solution.py:39
  102.9 0.6 copy.37
  (11 shorter events, 0.2 us)
Async XLA Ops:
  0.6 3.8 %copy-start = (bf16[24,64,1024]{2,1,0:T(8,128)(2,1)S(1)}, bf16[24,64,1024]{2,1,0:T(8,128)(2,1)}, u32[]{:S(2)}) copy-start(bf16[24,64,1024]{2,1,0:T(8,128)(2,1)} %param.22) | copy-start | bytes 9437188
  1.7 0.5 copy-start.9
  4.4 2.4 %copy-start.3 = (pred[24,1024]{1,0:T(8,128)(4,1)}, pred[24,1024]{1,0:T(8,128)(4,1)S(1)}, u32[]{:S(2)}) copy-start(pred[24,1024]{1,0:T(8,128)(4,1)S(1)} %iota_compare_fusion) | copy-start | bytes 73732
  14.0 13.5 %copy-start.1 = (bf16[24,1024]{1,0:T(8,128)(2,1)S(1)}, bf16[24,1024]{1,0:T(8,128)(2,1)}, u32[]{:S(2)}) copy-start(bf16[24,1024]{1,0:T(8,128)(2,1)} %param.16) | copy-start | bytes 147460
  14.0 14.3 %copy-start.5 = (f32[1024]{0:T(1024)S(1)}, f32[1024]{0:T(1024)}, u32[]{:S(2)}) copy-start(f32[1024]{0:T(1024)} %param.26) | copy-start | bytes 12292
  14.0 14.4 %copy-start.8 = (s32[24,2]{0,1:T(2,128)S(1)}, s32[24,2]{0,1:T(2,128)}, u32[]{:S(2)}) copy-start(s32[24,2]{0,1:T(2,128)} %param.27) | copy-start | bytes 580
  27.6 0.6 copy-start.2
  28.9 0.5 copy-start.6
  30.4 25.5 %all-to-all-start = ((bf16[64,2,1024]{2,1,0:T(2,128)(2,1)}), bf16[64,2,1024]{2,1,0:T(2,128)(2,1)}, u32[]{:S(2)}, u32[]{:S(2)}) async-start(bf16[64,2,1024]{2,1,0:T(2,128)(2,1)} %reshape.182), calls=%async_computation | async-start | bytes 524288 | tf_op jit(solution)/shard_map/all_to_all | solution.py:145
  59.7 11.0 %copy-start.7 = (s32[48]{0:T(128)S(1)}, s32[48]{0:T(128)}, u32[]{:S(2)}) copy-start(s32[48]{0:T(128)} %copy-done.6) | copy-start | bytes 580
  59.7 21.8 %copy-start.4 = (f32[1024]{0:T(1024)S(1)}, f32[1024]{0:T(1024)}, u32[]{:S(2)}) copy-start(f32[1024]{0:T(1024)} %param.17) | copy-start | bytes 12292
  59.7 21.8 %copy-start.10 = (f32[24]{0:T(128)S(1)}, f32[24]{0:T(128)}, u32[]{:S(2)}) copy-start(f32[24]{0:T(128)} %copy-done.9) | copy-start | bytes 292
  63.5 29.1 %copy-start.11 = (f32[24,2]{0,1:T(2,128)S(1)}, f32[24,2]{0,1:T(2,128)}, u32[]{:S(2)}) copy-start(f32[24,2]{0,1:T(2,128)} %param.28) | copy-start | bytes 580
  65.1 10.6 %all-to-all-start.1 = ((bf16[4,128,256]{2,1,0:T(8,128)(2,1)}), bf16[4,128,256]{2,1,0:T(8,128)(2,1)S(1)}, u32[]{:S(2)}, u32[]{:S(2)}) async-start(bf16[4,128,256]{2,1,0:T(8,128)(2,1)} %bitcast.52), calls=%async_computation.1 | async-start | bytes 524288 | tf_op jit(solution)/shard_map/all_to_all | solution.py:27
  76.5 16.1 %all-to-all-start.2 = ((bf16[64,2,256]{2,1,0:T(2,128)(2,1)}), bf16[64,2,256]{2,1,0:T(2,128)(2,1)S(1)}, u32[]{:S(2)}, u32[]{:S(2)}) async-start(bf16[64,2,256]{2,1,0:T(2,128)(2,1)} %reshape.185), calls=%async_computation.2 | async-start | bytes 131072 | tf_op jit(solution)/shard_map/all_to_all | solution.py:153
  94.1 8.9 %all-to-all-start.3 = ((bf16[4,24,256]{2,1,0:T(8,128)(2,1)}), bf16[4,24,256]{2,1,0:T(8,128)(2,1)S(1)}, u32[]{:S(2)}, u32[]{:S(2)}) async-start(bf16[4,24,256]{2,1,0:T(8,128)(2,1)} %broadcast_in_dim.20), calls=%async_computation.3 | async-start | bytes 98304 | tf_op jit(solution)/shard_map/all_to_all | solution.py:39
where the time goes:
time: 104 us
  starting transfers between devices  29.1 us (28%)
  waiting for transfers between devices  28.5 us (27%)
  matrix products  21.5 us (21%)
  local copies, waits for them, and re-layouts  11.3 us (11%)
  blocking collectives  8.63 us (8%)
  other arithmetic  3.78 us (4%)
    all_to_all x1, starting transfers between devices, body(): lax.all_to_all(outgoing, 'ep', split_axis=0, concat_axis=0, tiled=True)  12.8 us
    all_to_all x1, waiting for transfers between devices, body(): lax.all_to_all(outgoing, 'ep', split_axis=0, concat_axis=0, tiled=True)  12.7 us
    all_to_all x1, waiting for transfers between devices, body(): lax.all_to_all(share_part.reshape(sources, slot_count, -1), 'ep', split_a...  9.33 us
    all_gather x1, blocking collectives, total_of_pieces(): return lax.all_gather(array, axis).astype(jnp.float32).sum(0)  8.63 us
    all_to_all x1, starting transfers between devices, copy_for_each(): return lax.all_to_all(copies, axis, split_axis=0, concat_axis=0, tiled=True)  5.64 us
    all_to_all x1, starting transfers between devices, sum_at_owner(): lax.all_to_all(tiles, axis, split_axis=0, concat_axis=0, tiled=True)  5.59 us
    all_to_all x1, starting transfers between devices, body(): lax.all_to_all(share_part.reshape(sources, slot_count, -1), 'ep', split_a...  5.03 us
    all_to_all x1, waiting for transfers between devices, sum_at_owner(): lax.all_to_all(tiles, axis, split_axis=0, concat_axis=0, tiled=True)  4.94 us
  transfers between devices with their start and end apart: 4, of which 4 were waited for; matrix products, arithmetic and copies ran while one was open for 3% of the time, Pallas kernels for 0%

commit v1 on v0

v1 whole, which is shorter than its diff:
```python
import jax
import jax.numpy as jnp
from jax import lax
from jax.experimental import pallas as pl
from jax.experimental.pallas import tpu as pltpu
from jax.sharding import PartitionSpec as P

MESH = pl.DeviceIdType.MESH
HEAD = 64
EPS = 1e-06
F32 = jnp.float32
BF16 = jnp.bfloat16


def rms(x, gain):
    factor = lax.rsqrt(jnp.mean(x * x, axis=-1, keepdims=True) + EPS)
    return (x * factor * gain).astype(BF16)


def iota(shape, dim):
    return lax.broadcasted_iota(jnp.int32, shape, dim)


def kernel(
    n_ep, n_tp,
    tok_h, again_h, wq_h, wk_h, wv_h, bias_h, key_h, val_h, len_h, wo_h, fgain_h, routes_h, rw_h, gate_h, up_h, down_h,
    mixed_o, nk_o, nv_o,
    tok, again, wq, wk, wv, bias, key, val, lens, wo, fgain, routes, rw, gate, up, down,
    tri, scores, part, part_in, disp, disp_in, back, back_in, fin, fin_in, wide, rows, hidden,
    in_sem, send_sem, recv_sem,
):
    ep, tp = lax.axis_index("ep"), lax.axis_index("tp")
    seqs, width = tok.shape
    groups = seqs // 8

    def load(n, src, dst):
        copy = pltpu.make_async_copy(src, dst, in_sem.at[n])
        copy.start()
        return copy

    c_tok = load(0, tok_h, tok)
    c_again = load(1, again_h, again)
    c_wq = load(2, wq_h, wq)
    c_bias = load(3, bias_h, bias)
    c_len = load(4, len_h, lens)
    c_key = [load(5 + g, key_h.at[pl.ds(8 * g, 8)], key.at[pl.ds(8 * g, 8)]) for g in range(groups)]
    c_val = [load(8 + g, val_h.at[pl.ds(8 * g, 8)], val.at[pl.ds(8 * g, 8)]) for g in range(groups)]
    c_wo = load(11, wo_h, wo)
    c_fgain = load(12, fgain_h, fgain)
    c_routes = load(13, routes_h, routes)
    c_rw = load(14, rw_h, rw)
    c_wk = load(15, wk_h, wk)
    c_wv = load(16, wv_h, wv)

    barrier = pltpu.get_barrier_semaphore()

    def greet_ep(i, carry):
        pl.semaphore_signal(barrier, inc=1, device_id=(lax.rem(ep + i, n_ep), tp), device_id_type=MESH)
        return carry

    def greet_tp(i, carry):
        pl.semaphore_signal(barrier, inc=1, device_id=(ep, lax.rem(tp + i, n_tp)), device_id_type=MESH)
        return carry

    lax.fori_loop(1, n_ep, greet_ep, 0)
    lax.fori_loop(1, n_tp, greet_tp, 0)

    tri[...] = jnp.where(iota((512, 256), 0) >= iota((512, 256), 1), 1.0, 0.0).astype(BF16)

    lane, sub = iota((8, 128), 1), iota((8, 128), 0)
    low = lane < 64
    own = [sub == 2 * j + jnp.where(low, 0, 1) for j in range(4)]

    c_tok.wait()
    c_again.wait()
    tokens = tok[...].astype(F32)
    normed = rms(tokens, again[...])
    c_wq.wait()
    queries = jnp.dot(normed, wq[...], preferred_element_type=F32).astype(BF16).astype(F32)

    c_bias.wait()
    c_len.wait()
    c_gate = load(17, gate_h.at[0], gate)
    c_up = load(18, up_h.at[0], up)
    c_down = load(19, down_h.at[0], down)

    for g in range(groups):
        blocks = []
        for h in range(4):
            half = queries[8 * g : 8 * g + 8, 128 * (h // 2) : 128 * (h // 2) + 128]
            turned = pltpu.roll(half, 64, 1)
            both = jnp.where(low, half, turned) if h % 2 == 0 else jnp.where(low, turned, half)
            blocks.append(jnp.concatenate([jnp.where(own[j], both, 0.0) for j in range(4)], axis=1))
        spread = jnp.concatenate(blocks, axis=0).astype(BF16)
        c_key[g].wait()
        raw = jnp.dot(spread, key[pl.ds(8 * g, 8)].reshape(512, 1024), preferred_element_type=F32)
        for h in range(4):
            scores[pl.ds(32 * g + 8 * h, 8), :] = raw[8 * h : 8 * h + 8] * HEAD**-0.5 + bias[h]

    position = iota((32, 1024), 1)
    attended = []
    for g in range(groups):
        s = scores[pl.ds(32 * g, 32), :]
        length = jnp.zeros((8, 128), jnp.int32)
        for r in range(8):
            length = jnp.where(sub == r, lens[8 * g + r], length)
        length = jnp.concatenate([length] * 8, axis=1)
        length = jnp.concatenate([length] * 4, axis=0)
        inside = position < length
        fall = jnp.where(inside, -(jnp.maximum(s, 0.0) + jnp.log(1.0 + jnp.exp(-jnp.abs(s)))), 0.0)
        pieces = [fall[:, 256 * b : 256 * b + 256] for b in range(4)]
        later = [None] * 4
        later[3] = jnp.zeros_like(pieces[3])
        for b in (2, 1, 0):
            later[b] = later[b + 1] + pieces[b + 1]
        stacked = jnp.concatenate([jnp.concatenate([pieces[b], later[b]], axis=1) for b in range(4)], axis=0)
        high = stacked.astype(BF16)
        rest = (stacked - high.astype(F32)).astype(BF16)
        total = jnp.dot(high, tri[...], preferred_element_type=F32) + jnp.dot(rest, tri[...], preferred_element_type=F32)
        total = jnp.concatenate([total[32 * b : 32 * b + 32] for b in range(4)], axis=1)
        weights = jnp.where(inside, jnp.exp(s + total), 0.0).astype(BF16)
        c_val[g].wait()
        mixed = lax.dot_general(
            weights, val[pl.ds(8 * g, 8)].reshape(512, 1024), (((1,), (1,)), ((), ())), preferred_element_type=F32
        )
        heads = []
        for h in range(4):
            m = [jnp.where(own[j], mixed[8 * h : 8 * h + 8, 128 * j : 128 * j + 128], 0.0) for j in range(4)]
            m = (m[0] + m[1]) + (m[2] + m[3])
            heads.append(m + pltpu.roll(m, 64, 1))
        attended.append(jnp.concatenate([jnp.where(low, heads[0], heads[1]), jnp.where(low, heads[2], heads[3])], axis=1))
    attended = jnp.concatenate(attended, axis=0).astype(BF16)
    c_wo.wait()
    part[...] = jnp.dot(attended, wo[...], preferred_element_type=F32).astype(BF16)

    pl.semaphore_wait(barrier, n_ep + n_tp - 2)

    def to_tp(src, dst, n):
        def send(i, carry):
            pltpu.make_async_remote_copy(
                src_ref=src, dst_ref=dst.at[tp], send_sem=send_sem.at[n], recv_sem=recv_sem.at[n],
                device_id=(ep, lax.rem(tp + i, n_tp)), device_id_type=MESH,
            ).start()
            return carry

        lax.fori_loop(1, n_tp, send, 0)

    def to_ep(src, dst, n):
        def send(i, carry):
            p = lax.rem(ep + i, n_ep)
            pltpu.make_async_remote_copy(
                src_ref=src.at[p], dst_ref=dst.at[ep], send_sem=send_sem.at[n], recv_sem=recv_sem.at[n],
                device_id=(p, tp), device_id_type=MESH,
            ).start()
            return carry

        lax.fori_loop(1, n_ep, send, 0)

    def arrived(dst, n, count, sems):
        some = dst.at[pl.ds(0, count)]
        pltpu.make_async_copy(some, some, sems.at[n]).wait()

    to_tp(part, part_in, 0)
    part_in[tp] = part[...]

    c_routes.wait()
    c_rw.wait()
    c_fgain.wait()
    lane24 = iota((seqs, 128), 1)
    expert = lane24 - jnp.where(lane24 >= n_ep, n_ep, 0)
    slot = jnp.where(lane24 >= n_ep, 1.0, 0.0)
    first = jnp.where(routes[:, 0:1] == expert, 1.0, 0.0)
    second = jnp.where(routes[:, 1:2] == expert, 1.0, 0.0)
    chosen = first + second
    below = jnp.where(iota((seqs, seqs), 0) > iota((seqs, seqs), 1), 1.0, 0.0)
    before = jnp.dot(below.astype(BF16), chosen.astype(BF16), preferred_element_type=F32)
    here = jnp.where(before == slot, 1.0, 0.0)
    plan = jnp.transpose(chosen * here).astype(BF16)
    gather = (first * rw[:, 0:1] + second * rw[:, 1:2]) * here
    gather_high = gather.astype(BF16)
    gather_rest = (gather - gather_high.astype(F32)).astype(BF16)
    c_wk.wait()
    nk_o[...] = jnp.dot(normed, wk[...], preferred_element_type=F32).astype(BF16)
    c_wv.wait()
    nv_o[...] = jnp.dot(normed, wv[...], preferred_element_type=F32).astype(BF16)

    arrived(part_in, 0, n_tp - 1, recv_sem)
    summed = part_in[0].astype(F32)
    for t in range(1, n_tp):
        summed = summed + part_in[t].astype(F32)
    residual = (tokens + summed).astype(BF16).astype(F32)
    normed_two = rms(residual, fgain[...])

    def store_rows(j, both):
        for s in range(2):
            wide[pl.ds(8 * s + j, n_ep, stride=16), :] = both[n_ep * s : n_ep * (s + 1)]

    def read_rows(j):
        return jnp.concatenate([wide[pl.ds(8 * s + j, n_ep, stride=16), :] for s in range(2)], axis=0)

    for j in range(8):
        store_rows(j, jnp.dot(plan, normed_two[:, 128 * j : 128 * j + 128], preferred_element_type=F32))
    disp[...] = wide[...].astype(BF16).reshape(n_ep, 16, 128)
    to_ep(disp, disp_in, 1)
    disp_in[ep] = disp[ep]

    c_gate.wait()
    c_up.wait()
    c_down.wait()
    arrived(disp_in, 1, n_ep - 1, recv_sem)
    wide[...] = disp_in[...].astype(F32).reshape(n_ep * 16, 128)
    for j in range(8):
        rows[:, 128 * j : 128 * j + 128] = read_rows(j).astype(BF16)

    units = gate.shape[1]
    for c in range(0, units, 256):
        size = min(256, units - c)
        a = jnp.dot(rows[...], gate[:, c : c + size], preferred_element_type=F32)
        b = jnp.dot(rows[...], up[:, c : c + size], preferred_element_type=F32)
        hidden[:, c : c + size] = (a / (1.0 + jnp.exp(-a)) * b).astype(BF16)
    for c in range(0, width, 256):
        out = jnp.dot(hidden[...], down[:, c : c + 256], preferred_element_type=F32)
        for i in range(2):
            store_rows(c // 128 + i, out[:, 128 * i : 128 * i + 128])
    back[...] = wide[...].astype(BF16).reshape(n_ep, 16, 128)
    to_ep(back, back_in, 2)
    back_in[ep] = back[ep]

    arrived(back_in, 2, n_ep - 1, recv_sem)
    wide[...] = back_in[...].astype(F32).reshape(n_ep * 16, 128)
    for j in range(8):
        rows[:, 128 * j : 128 * j + 128] = read_rows(j).astype(BF16)
    fin[...] = (
        jnp.dot(gather_high, rows[...], preferred_element_type=F32)
        + jnp.dot(gather_rest, rows[...], preferred_element_type=F32)
    ).astype(BF16)
    to_tp(fin, fin_in, 3)
    fin_in[tp] = fin[...]
    arrived(part_in, 0, n_tp - 1, send_sem)
    arrived(disp_in, 1, n_ep - 1, send_sem)
    arrived(back_in, 2, n_ep - 1, send_sem)
    arrived(fin_in, 3, n_tp - 1, recv_sem)
    summed = fin_in[0].astype(F32)
    for t in range(1, n_tp):
        summed = summed + fin_in[t].astype(F32)
    mixed_o[...] = (residual + summed).astype(BF16)
    arrived(fin_in, 3, n_tp - 1, send_sem)


def solution(mesh):
    n_ep, n_tp = mesh.shape["ep"], mesh.shape["tp"]

    def body(*args):
        (tokens, attn_gain, w_query, w_key, w_value, attn_bias, key_cache, value_cache, lengths, w_out,
         ffn_gain, routes, route_weight, expert_gate, expert_up, expert_down) = args
        seqs, width = tokens.shape
        units = expert_gate.shape[2]
        operands = (
            tokens, attn_gain.reshape(1, width), w_query, w_key, w_value, attn_bias, key_cache, value_cache, lengths,
            w_out, ffn_gain.reshape(1, width), routes, route_weight, expert_gate, expert_up, expert_down,
        )
        vmem, smem = pltpu.VMEM, pltpu.SMEM

        def run(*refs):
            kernel(n_ep, n_tp, *refs)

        return pl.pallas_call(
            run,
            name="layer",
            out_shape=(
                jax.ShapeDtypeStruct(tokens.shape, BF16),
                jax.ShapeDtypeStruct((seqs, w_key.shape[1]), BF16),
                jax.ShapeDtypeStruct((seqs, w_value.shape[1]), BF16),
            ),
            in_specs=[pl.BlockSpec(memory_space=pltpu.HBM)] * len(operands),
            out_specs=(pl.BlockSpec(memory_space=vmem),) * 3,
            scratch_shapes=[
                vmem(tokens.shape, BF16), vmem((1, width), F32), vmem(w_query.shape, BF16), vmem(w_key.shape, BF16),
                vmem(w_value.shape, BF16), smem(attn_bias.shape, F32), vmem(key_cache.shape, BF16),
                vmem(value_cache.shape, BF16), smem(lengths.shape, jnp.int32), vmem(w_out.shape, BF16),
                vmem((1, width), F32), vmem(routes.shape, jnp.int32), vmem(route_weight.shape, F32),
                vmem(expert_gate.shape[1:], BF16), vmem(expert_up.shape[1:], BF16), vmem(expert_down.shape[1:], BF16),
                vmem((512, 256), BF16), vmem((4 * seqs, 1024), F32), vmem(tokens.shape, BF16),
                vmem((n_tp, seqs, width), BF16), vmem((n_ep, 16, 128), BF16), vmem((n_ep, 16, 128), BF16),
                vmem((n_ep, 16, 128), BF16), vmem((n_ep, 16, 128), BF16), vmem(tokens.shape, BF16),
                vmem((n_tp, seqs, width), BF16), vmem((n_ep * 16, 128), F32), vmem((2 * n_ep, width), BF16),
                vmem((2 * n_ep, units), BF16),
                pltpu.SemaphoreType.DMA((20,)), pltpu.SemaphoreType.DMA((4,)), pltpu.SemaphoreType.DMA((4,)),
            ],
            compiler_params=pltpu.CompilerParams(
                collective_id=0, has_side_effects=True, vmem_limit_bytes=48 * 1024 * 1024
            ),
        )(*operands)

    return jax.shard_map(
        body,
        mesh=mesh,
        in_specs=(
            P("ep", None), P(), P(None, "tp"), P(None, "tp"), P(None, "tp"), P("tp"), P("ep", "tp", None),
            P("ep", "tp", None), P("ep"), P("tp", None), P(), P("ep", None), P("ep", None), P("ep", None, "tp"),
            P("ep", None, "tp"), P("ep", "tp", None),
        ),
        out_specs=(P("ep", None), P("ep", "tp"), P("ep", "tp")),
        check_vma=False,
    )
```

time: 104 us -> 59.3 us (0.57)
  Pallas kernels: 0 us -> 44.1 us
  starting transfers between devices: 29.1 us -> 0 us
  waiting for transfers between devices: 28.5 us -> 0 us
  matrix products: 21.5 us -> 0 us
  blocking collectives: 8.63 us -> 0 us
  other arithmetic: 3.78 us -> 0 us
  local copies, waits for them, and re-layouts: 11.3 us -> 14 us
    pallas_call x0 -> x1, Pallas kernels: none -> 44.1 us  [body(): pl.pallas_call(run, name='layer', out_shape=(jax.ShapeDtypeStruct(tokens....]
    all_to_all x4 -> x0, starting transfers between devices: 29.1 us -> none  [the longest x1 12.8 us: body(): lax.all_to_all(outgoing, 'ep', split_axis=0, concat_axis=0, tiled=True)]
    all_to_all x4 -> x0, waiting for transfers between devices: 28.5 us -> none  [the longest x1 12.7 us: body(): lax.all_to_all(outgoing, 'ep', split_axis=0, concat_axis=0, tiled=True)]
    dot_general x13 -> x0, matrix products: 21.5 us -> none  [the longest x1 3.73 us: body(): jnp.dot(hidden, down_local, preferred_element_type=jnp.float32)]
    unnamed x25, local copies, waits for them, and re-layouts: 1.75 us -> 14 us
    all_gather x1 -> x0, blocking collectives: 8.63 us -> none  [total_of_pieces(): return lax.all_gather(array, axis).astype(jnp.float32).sum(0)]
    reshape x10 -> x0, local copies, waits for them, and re-layouts: 6.9 us -> none  [the longest x1 1.86 us: suffix_totals(): return (within + later[..., None]).reshape(lead_shape + (key_span,))]
    reduce_sum x5 -> x0, other arithmetic: 2.09 us -> none  [the longest x2 1.2 us: rms_scale(): jnp.mean(widened * widened, axis=-1, keepdims=True) + norm_epsilon]
  transfers between devices with their start and end apart: 4 -> 0, of which waited for: 4 -> 0; matrix products, arithmetic and copies ran while one was open for 3% -> 0% of each run, Pallas kernels for 0% -> 0%
where the time goes in v1:
time: 59.3 us; the launch traced here: 58.8 us
  Pallas kernels  44.1 us (74%)
  local copies, waits for them, and re-layouts  14 us (24%)
  between operations  0.67 us (1%)
    pallas_call x1, Pallas kernels, body(): pl.pallas_call(run, name='layer', out_shape=(jax.ShapeDtypeStruct(tokens....  44.1 us
    unnamed x25, local copies, waits for them, and re-layouts  14 us

profile of v1, /device:TPU:1, one launch (start us, length us, event | category | flops | bytes accessed | tf_op | source)
XLA Modules:
  0.0 58.8 jit_solution(15712992351756534869)
XLA Ops:
  0.6 0.8 %copy.21.refs_11_ = s32[24,2]{1,0:T(8,128)S(1)} copy(s32[24,2]{0,1:T(2,128)} %param.27) | data formatting | bytes 384 | tf_op args[11]
  1.4 0.8 %copy.22.refs_12_ = f32[24,2]{1,0:T(8,128)S(1)} copy(f32[24,2]{0,1:T(2,128)} %param.28) | data formatting | bytes 384 | tf_op args[12]
  2.1 1.1 %copy.19.refs_3_ = bf16[1024,64]{1,0:T(8,128)(2,1)S(1)} copy(bf16[1024,64]{0,1:T(8,128)(2,1)} %param.19) | data formatting | bytes 262144 | tf_op args[3]
  3.2 1.1 %copy.20.refs_4_ = bf16[1024,64]{1,0:T(8,128)(2,1)S(1)} copy(bf16[1024,64]{0,1:T(8,128)(2,1)} %param.20) | data formatting | bytes 262144 | tf_op args[4]
  4.3 0.0 copy-start
  4.3 1.5 %copy-done = bf16[1,1024,896]{2,1,0:T(8,128)(2,1)S(1)} copy-done((bf16[1,1024,896]{2,1,0:T(8,128)(2,1)S(1)}, bf16[1,1024,896]{2,1,0:T(8,128)(2,1)}, u32[]{:S(2)}) %copy-start) | copy-done | bytes 1835032
  5.8 0.0 copy-start.1
  5.8 1.5 %copy-done.1 = bf16[1,1024,896]{2,1,0:T(8,128)(2,1)S(1)} copy-done((bf16[1,1024,896]{2,1,0:T(8,128)(2,1)S(1)}, bf16[1,1024,896]{2,1,0:T(8,128)(2,1)}, u32[]{:S(2)}) %copy-start.1) | copy-done | bytes 1835032
  7.3 0.0 copy-start.2
  7.3 1.0 %copy-done.2 = bf16[1024,256]{1,0:T(8,128)(2,1)S(1)} copy-done((bf16[1024,256]{1,0:T(8,128)(2,1)S(1)}, bf16[1024,256]{1,0:T(8,128)(2,1)}, u32[]{:S(2)}) %copy-start.2) | copy-done | bytes 524312
  8.4 0.0 copy-start.3
  8.4 1.0 %copy-done.3 = bf16[256,1024]{1,0:T(8,128)(2,1)S(1)} copy-done((bf16[256,1024]{1,0:T(8,128)(2,1)S(1)}, bf16[256,1024]{1,0:T(8,128)(2,1)}, u32[]{:S(2)}) %copy-start.3) | copy-done | bytes 524312
  9.4 0.0 copy-start.4
  9.4 0.8 %copy-done.4 = bf16[24,1024]{1,0:T(8,128)(2,1)S(1)} copy-done((bf16[24,1024]{1,0:T(8,128)(2,1)S(1)}, bf16[24,1024]{1,0:T(8,128)(2,1)}, u32[]{:S(2)}) %copy-start.4) | copy-done | bytes 49176
  10.2 0.0 copy-start.5
  10.2 0.7 %copy-done.5 = f32[1024]{0:T(1024)S(1)} copy-done((f32[1024]{0:T(1024)S(1)}, f32[1024]{0:T(1024)}, u32[]{:S(2)}) %copy-start.5) | copy-done | bytes 4120
  10.9 0.0 copy-start.6
  10.9 0.7 %copy-done.6 = f32[1024]{0:T(1024)S(1)} copy-done((f32[1024]{0:T(1024)S(1)}, f32[1024]{0:T(1024)}, u32[]{:S(2)}) %copy-start.6) | copy-done | bytes 4120
  11.6 0.0 copy-start.7
  11.6 0.7 %copy-done.7 = f32[4]{0:T(128)S(1)} copy-done((f32[4]{0:T(128)S(1)}, f32[4]{0:T(128)}, u32[]{:S(2)}) %copy-start.7) | copy-done | bytes 40
  12.2 0.0 copy-start.8
  12.2 0.7 %copy-done.8 = s32[24]{0:T(128)S(1)} copy-done((s32[24]{0:T(128)S(1)}, s32[24]{0:T(128)}, u32[]{:S(2)}) %copy-start.8) | copy-done | bytes 120
  12.9 44.1 %layer.1 = (bf16[24,1024]{1,0:T(8,128)(2,1)S(1)}, bf16[24,64]{1,0:T(8,128)(2,1)S(1)}, bf16[24,64]{1,0:T(8,128)(2,1)S(1)}) custom-call(bf16[24,1024]{1,0:T(8,128)(2,1)S(1)} %copy-done.4, f32[1,1024]{1,0:T(1,128)S(1)} %bitcast.2, bf16[1024,256]{1,0:T(8,128)(2,1)S(1)} %copy-done.2, bf16[1024,64]{1,0:T(8,128)(2,1)S(1)} %copy.19.refs_3_, ...), custom_call_target="tpu_custom_call" | custom-call | tf_op jit(solution)/shard_map/layer/pallas_call | solution.py:267
  57.0 0.6 %copy.26 = bf16[24,1024]{1,0:T(8,128)(2,1)} copy(bf16[24,1024]{1,0:T(8,128)(2,1)S(1)} %get-tuple-element.6) | data formatting | bytes 98304
  57.6 0.6 %copy.27 = bf16[24,64]{1,0:T(8,128)(2,1)} copy(bf16[24,64]{1,0:T(8,128)(2,1)S(1)} %get-tuple-element.7) | data formatting | bytes 6144
  58.2 0.6 %copy.28 = bf16[24,64]{1,0:T(8,128)(2,1)} copy(bf16[24,64]{1,0:T(8,128)(2,1)S(1)} %get-tuple-element.8) | data formatting | bytes 6144
Async XLA Ops:
  4.3 1.5 %copy-start = (bf16[1,1024,896]{2,1,0:T(8,128)(2,1)S(1)}, bf16[1,1024,896]{2,1,0:T(8,128)(2,1)}, u32[]{:S(2)}) copy-start(bf16[1,1024,896]{2,1,0:T(8,128)(2,1)} %refs_13_.1) | copy-start | bytes 5505028
  5.8 1.5 %copy-start.1 = (bf16[1,1024,896]{2,1,0:T(8,128)(2,1)S(1)}, bf16[1,1024,896]{2,1,0:T(8,128)(2,1)}, u32[]{:S(2)}) copy-start(bf16[1,1024,896]{2,1,0:T(8,128)(2,1)} %refs_14_.1) | copy-start | bytes 5505028
  7.3 1.0 %copy-start.2 = (bf16[1024,256]{1,0:T(8,128)(2,1)S(1)}, bf16[1024,256]{1,0:T(8,128)(2,1)}, u32[]{:S(2)}) copy-start(bf16[1024,256]{1,0:T(8,128)(2,1)} %refs_2_.1) | copy-start | bytes 1572868
  8.4 1.0 %copy-start.3 = (bf16[256,1024]{1,0:T(8,128)(2,1)S(1)}, bf16[256,1024]{1,0:T(8,128)(2,1)}, u32[]{:S(2)}) copy-start(bf16[256,1024]{1,0:T(8,128)(2,1)} %refs_9_.1) | copy-start | bytes 1572868
  9.4 0.8 %copy-start.4 = (bf16[24,1024]{1,0:T(8,128)(2,1)S(1)}, bf16[24,1024]{1,0:T(8,128)(2,1)}, u32[]{:S(2)}) copy-start(bf16[24,1024]{1,0:T(8,128)(2,1)} %refs_0_.1) | copy-start | bytes 147460
  10.2 0.7 %copy-start.5 = (f32[1024]{0:T(1024)S(1)}, f32[1024]{0:T(1024)}, u32[]{:S(2)}) copy-start(f32[1024]{0:T(1024)} %param.17) | copy-start | bytes 12292
  10.9 0.7 %copy-start.6 = (f32[1024]{0:T(1024)S(1)}, f32[1024]{0:T(1024)}, u32[]{:S(2)}) copy-start(f32[1024]{0:T(1024)} %param.26) | copy-start | bytes 12292
  11.6 0.7 %copy-start.7 = (f32[4]{0:T(128)S(1)}, f32[4]{0:T(128)}, u32[]{:S(2)}) copy-start(f32[4]{0:T(128)} %refs_5_.1) | copy-start | bytes 52
  12.2 0.7 %copy-start.8 = (s32[24]{0:T(128)S(1)}, s32[24]{0:T(128)}, u32[]{:S(2)}) copy-start(s32[24]{0:T(128)} %refs_8_.1) | copy-start | bytes 292

commit v2 on v1

--- a/solution.py
+++ b/solution.py
@@ -1,3 +1,5 @@
+import random
+
 import jax
 import jax.numpy as jnp
 from jax import lax
@@ -8,6 +10,7 @@
 MESH = pl.DeviceIdType.MESH
 HEAD = 64
 EPS = 1e-06
+Z, Y, X = 8, 4, 2
 F32 = jnp.float32
 BF16 = jnp.bfloat16
 
@@ -19,6 +22,12 @@
 
 def iota(shape, dim):
     return lax.broadcasted_iota(jnp.int32, shape, dim)
+
+
+def far_first():
+    offsets = [(z, y, x) for z in range(Z) for y in range(Y) for x in range(X)][1:]
+    random.Random(0).shuffle(offsets)
+    return sorted(offsets, key=lambda o: -(min(o[0], Z - o[0]) + min(o[1], Y - o[1]) + 2 * o[2]))
 
 
 def kernel(
@@ -30,6 +39,7 @@
     in_sem, send_sem, recv_sem,
 ):
     ep, tp = lax.axis_index("ep"), lax.axis_index("tp")
+    z, y, x = ep // (Y * X), lax.rem(ep // X, Y), lax.rem(ep, X)
     seqs, width = tok.shape
     groups = seqs // 8
 
@@ -146,15 +156,12 @@
         lax.fori_loop(1, n_tp, send, 0)
 
     def to_ep(src, dst, n):
-        def send(i, carry):
-            p = lax.rem(ep + i, n_ep)
+        for dz, dy, dx in far_first():
+            p = (lax.rem(z + dz, Z) * Y + lax.rem(y + dy, Y)) * X + lax.rem(x + dx, X)
             pltpu.make_async_remote_copy(
                 src_ref=src.at[p], dst_ref=dst.at[ep], send_sem=send_sem.at[n], recv_sem=recv_sem.at[n],
                 device_id=(p, tp), device_id_type=MESH,
             ).start()
-            return carry
-
-        lax.fori_loop(1, n_ep, send, 0)
 
     def arrived(dst, n, count, sems):
         some = dst.at[pl.ds(0, count)]
@@ -166,23 +173,24 @@
     c_routes.wait()
     c_rw.wait()
     c_fgain.wait()
-    lane24 = iota((seqs, 128), 1)
-    expert = lane24 - jnp.where(lane24 >= n_ep, n_ep, 0)
-    slot = jnp.where(lane24 >= n_ep, 1.0, 0.0)
-    first = jnp.where(routes[:, 0:1] == expert, 1.0, 0.0)
-    second = jnp.where(routes[:, 1:2] == expert, 1.0, 0.0)
+    place = iota((2 * n_ep, seqs), 0)
+    expert = place - jnp.where(place >= n_ep, n_ep, 0)
+    slot = jnp.where(place >= n_ep, 1.0, 0.0)
+    first = jnp.where(routes[0:1, :] == expert, 1.0, 0.0)
+    second = jnp.where(routes[1:2, :] == expert, 1.0, 0.0)
     chosen = first + second
-    below = jnp.where(iota((seqs, seqs), 0) > iota((seqs, seqs), 1), 1.0, 0.0)
-    before = jnp.dot(below.astype(BF16), chosen.astype(BF16), preferred_element_type=F32)
+    above = jnp.where(iota((seqs, seqs), 0) < iota((seqs, seqs), 1), 1.0, 0.0)
+    before = jnp.dot(chosen.astype(BF16), above.astype(BF16), preferred_element_type=F32)
     here = jnp.where(before == slot, 1.0, 0.0)
-    plan = jnp.transpose(chosen * here).astype(BF16)
-    gather = (first * rw[:, 0:1] + second * rw[:, 1:2]) * here
+    plan = (chosen * here).astype(BF16)
+    gather = jnp.transpose((first * rw[0:1, :] + second * rw[1:2, :]) * here)
     gather_high = gather.astype(BF16)
     gather_rest = (gather - gather_high.astype(F32)).astype(BF16)
+    turned = (((1,), (1,)), ((), ()))
     c_wk.wait()
-    nk_o[...] = jnp.dot(normed, wk[...], preferred_element_type=F32).astype(BF16)
+    nk_o[...] = lax.dot_general(normed, wk[...], turned, preferred_element_type=F32).astype(BF16)
     c_wv.wait()
-    nv_o[...] = jnp.dot(normed, wv[...], preferred_element_type=F32).astype(BF16)
+    nv_o[...] = lax.dot_general(normed, wv[...], turned, preferred_element_type=F32).astype(BF16)
 
     arrived(part_in, 0, n_tp - 1, recv_sem)
     summed = part_in[0].astype(F32)
@@ -247,6 +255,15 @@
     arrived(fin_in, 3, n_tp - 1, send_sem)
 
 
+def write_out(*refs):
+    ins, outs, sems = refs[:3], refs[3:6], refs[6]
+    copies = [pltpu.make_async_copy(ins[i], outs[i], sems.at[i]) for i in range(3)]
+    for copy in copies:
+        copy.start()
+    for copy in copies:
+        copy.wait()
+
+
 def solution(mesh):
     n_ep, n_tp = mesh.shape["ep"], mesh.shape["tp"]
 
@@ -256,15 +273,15 @@
         seqs, width = tokens.shape
         units = expert_gate.shape[2]
         operands = (
-            tokens, attn_gain.reshape(1, width), w_query, w_key, w_value, attn_bias, key_cache, value_cache, lengths,
-            w_out, ffn_gain.reshape(1, width), routes, route_weight, expert_gate, expert_up, expert_down,
+            tokens, attn_gain.reshape(1, width), w_query, w_key.T, w_value.T, attn_bias, key_cache, value_cache, lengths,
+            w_out, ffn_gain.reshape(1, width), routes.T, route_weight.T, expert_gate, expert_up, expert_down,
         )
         vmem, smem = pltpu.VMEM, pltpu.SMEM
 
         def run(*refs):
             kernel(n_ep, n_tp, *refs)
 
-        return pl.pallas_call(
+        results = pl.pallas_call(
             run,
             name="layer",
             out_shape=(
@@ -275,10 +292,10 @@
             in_specs=[pl.BlockSpec(memory_space=pltpu.HBM)] * len(operands),
             out_specs=(pl.BlockSpec(memory_space=vmem),) * 3,
             scratch_shapes=[
-                vmem(tokens.shape, BF16), vmem((1, width), F32), vmem(w_query.shape, BF16), vmem(w_key.shape, BF16),
-                vmem(w_value.shape, BF16), smem(attn_bias.shape, F32), vmem(key_cache.shape, BF16),
+                vmem(tokens.shape, BF16), vmem((1, width), F32), vmem(w_query.shape, BF16), vmem(w_key.shape[::-1], BF16),
+                vmem(w_value.shape[::-1], BF16), smem(attn_bias.shape, F32), vmem(key_cache.shape, BF16),
                 vmem(value_cache.shape, BF16), smem(lengths.shape, jnp.int32), vmem(w_out.shape, BF16),
-                vmem((1, width), F32), vmem(routes.shape, jnp.int32), vmem(route_weight.shape, F32),
+                vmem((1, width), F32), vmem(routes.shape[::-1], jnp.int32), vmem(route_weight.shape[::-1], F32),
                 vmem(expert_gate.shape[1:], BF16), vmem(expert_up.shape[1:], BF16), vmem(expert_down.shape[1:], BF16),
                 vmem((512, 256), BF16), vmem((4 * seqs, 1024), F32), vmem(tokens.shape, BF16),
                 vmem((n_tp, seqs, width), BF16), vmem((n_ep, 16, 128), BF16), vmem((n_ep, 16, 128), BF16),
@@ -290,7 +307,17 @@
             compiler_params=pltpu.CompilerParams(
                 collective_id=0, has_side_effects=True, vmem_limit_bytes=48 * 1024 * 1024
             ),
-        )(*operands)
+        )(*[pltpu.with_memory_space_constraint(x, pltpu.HBM) for x in operands])
+
+        return pl.pallas_call(
+            write_out,
+            name="write_out",
+            out_shape=tuple(pltpu.HBM(r.shape, r.dtype) for r in results),
+            in_specs=[pl.BlockSpec(memory_space=vmem)] * 3,
+            out_specs=(pl.BlockSpec(memory_space=pltpu.HBM),) * 3,
+            scratch_shapes=[pltpu.SemaphoreType.DMA((3,))],
+            compiler_params=pltpu.CompilerParams(vmem_limit_bytes=1024 * 1024),
+        )(*[pltpu.with_memory_space_constraint(r, vmem) for r in results])
 
     return jax.shard_map(
         body,

time: 59.3 us -> 41.3 us (0.70)
  local copies, waits for them, and re-layouts: 14 us -> 0 us
  Pallas kernels: 44.1 us -> 40.6 us
    unnamed x25 -> x0, local copies, waits for them, and re-layouts: 14 us -> none
    pallas_call x1, Pallas kernels: 44.1 us -> 39.9 us  [body(): pl.pallas_call(run, name='layer', out_shape=(jax.ShapeDtypeStruct(tokens....]
    pallas_call x0 -> x1, Pallas kernels: none -> 0.65 us  [body(): pl.pallas_call(write_out, name='write_out', out_shape=tuple((pltpu.HBM(r....]
where the time goes in v2:
time: 41.3 us; the launch traced here: 41.2 us
  Pallas kernels  40.6 us (98%)
  between operations  0.65 us (2%)
    pallas_call x1, Pallas kernels, body(): pl.pallas_call(run, name='layer', out_shape=(jax.ShapeDtypeStruct(tokens....  39.9 us

profile of v2, /device:TPU:1, one launch (start us, length us, event | category | flops | bytes accessed | tf_op | source)
XLA Modules:
  0.0 41.2 jit_solution(11833741758466847323)
XLA Ops:
  0.6 39.9 %layer.1 = (bf16[24,1024]{1,0:T(8,128)(2,1)S(1)}, bf16[24,64]{1,0:T(8,128)(2,1)S(1)}, bf16[24,64]{1,0:T(8,128)(2,1)S(1)}) custom-call(bf16[24,1024]{1,0:T(8,128)(2,1)} %refs_0_.1, f32[1,1024]{1,0:T(1,128)} %bitcast.8, bf16[1024,256]{1,0:T(8,128)(2,1)} %refs_2_.1, bf16[64,1024]{1,0:T(8,128)(2,1)} %bitcast.6, bf16[64,1024]{1,0:T(8,128)(2,1)} %bitcast.7, ...), custom_call_target="tpu_custom_call" | custom-call | tf_op jit(solution)/shard_map/layer/pallas_call | solution.py:284
  40.5 0.7 %write_out.1 = (bf16[24,1024]{1,0:T(8,128)(2,1)}, bf16[24,64]{1,0:T(8,128)(2,1)}, bf16[24,64]{1,0:T(8,128)(2,1)}) custom-call(bf16[24,1024]{1,0:T(8,128)(2,1)S(1)} %get-tuple-element.6.refs_0_, bf16[24,64]{1,0:T(8,128)(2,1)S(1)} %get-tuple-element.7.refs_1_, bf16[24,64]{1,0:T(8,128)(2,1)S(1)} %get-tuple-element.8.refs_2_), custom_call_target="tpu_custom_call" | custom-call | tf_op jit(solution)/shard_map/write_out/pallas_call | solution.py:312

commit v3 on v2

v3 whole, which is shorter than its diff:
```python
import random

import jax
import jax.numpy as jnp
from jax import lax
from jax.experimental import pallas as pl
from jax.experimental.pallas import tpu as pltpu
from jax.sharding import PartitionSpec as P

MESH = pl.DeviceIdType.MESH
HEAD = 64
EPS = 1e-06
PARTS, FAR, NEAR, PAIR_FAR, PAIR_NEAR, PAIR_BACK, BACK, LAST, RESIDUAL = range(9)
Z, Y, X = 8, 4, 2
F32 = jnp.float32
BF16 = jnp.bfloat16


def rms(x, gain):
    factor = lax.rsqrt(jnp.mean(x * x, axis=-1, keepdims=True) + EPS)
    return (x * factor * gain).astype(BF16)


def iota(shape, dim):
    return lax.broadcasted_iota(jnp.int32, shape, dim)


def far_first():
    offsets = [(z, y, x) for z in range(Z) for y in range(Y) for x in range(X)][1:]
    random.Random(0).shuffle(offsets)
    return sorted(offsets, key=lambda o: -(min(o[0], Z - o[0]) + min(o[1], Y - o[1]) + 2 * o[2]))


def kernel(
    n_ep, n_tp,
    tok_h, again_h, wq_h, wk_h, wv_h, bias_h, key_h, val_h, len_h, wo_h, fgain_h, routes_h, rw_h, gate_h, up_h, down_h,
    mixed_o, nk_o, nv_o,
    tok, again, wq, wk, wv, bias, key, val, lens, wo, fgain, routes, rw, gate, up, down,
    tri, scores, falls_ref, part, part_in, disp, disp_in, disp_other, back, back_in, pair_out, pair_in, fin, fin_in, res_mine, res_other,
    wide, plain, rows, hidden,
    in_sem, send_sem, recv_sem,
):
    ep, tp = lax.axis_index("ep"), lax.axis_index("tp")
    z, y, x = ep // (Y * X), lax.rem(ep // X, Y), lax.rem(ep, X)
    zs = [lax.rem(z + d, Z) * (Y * X) for d in range(Z)]
    ys = [lax.rem(y + d, Y) * X for d in range(Y)]
    xs = [lax.rem(x + d, X) for d in range(X)]
    order = far_first()
    targets = [(zs[dz] + ys[dy]) + xs[dx] for dz, dy, dx in order]
    sources = [(zs[-dz % Z] + ys[-dy % Y]) + xs[-dx % X] for dz, dy, dx in order]
    core = lax.rem(tp, 2)
    partner = tp + 1 - 2 * core
    half_width = tok.shape[1] // 2
    far = n_ep // 2
    seqs, width = tok.shape
    groups = seqs // 8

    def load(n, src, dst):
        copy = pltpu.make_async_copy(src, dst, in_sem.at[n])
        copy.start()
        return copy

    c_tok = load(0, tok_h, tok)
    c_again = load(1, again_h, again)
    c_wq = load(2, wq_h, wq)
    c_bias = load(3, bias_h, bias)
    c_len = load(4, len_h, lens)
    c_key = [load(5 + g, key_h.at[pl.ds(8 * g, 8)], key.at[pl.ds(8 * g, 8)]) for g in range(groups)]
    c_val = [load(8 + g, val_h.at[pl.ds(8 * g, 8)], val.at[pl.ds(8 * g, 8)]) for g in range(groups)]
    c_wo = load(11, wo_h, wo)
    c_fgain = load(12, fgain_h, fgain)
    c_routes = load(13, routes_h, routes)
    c_rw = load(14, rw_h, rw)
    c_wk = load(15, wk_h, wk)
    c_wv = load(16, wv_h, wv)

    barrier = pltpu.get_barrier_semaphore()
    for p in targets:
        pl.semaphore_signal(barrier, inc=1, device_id=(p, tp), device_id_type=MESH)
    for i in range(1, n_tp):
        pl.semaphore_signal(barrier, inc=1, device_id=(ep, lax.rem(tp + i, n_tp)), device_id_type=MESH)

    tri[...] = jnp.where(iota((512, 256), 0) >= iota((512, 256), 1), 1.0, 0.0).astype(BF16)

    lane, sub = iota((8, 128), 1), iota((8, 128), 0)
    low = lane < 64
    own = [sub == 2 * j + jnp.where(low, 0, 1) for j in range(4)]

    c_tok.wait()
    c_again.wait()
    tokens = tok[...].astype(F32)
    normed = rms(tokens, again[...])
    c_wq.wait()
    queries = jnp.dot(normed, wq[...], preferred_element_type=F32).astype(BF16).astype(F32) * HEAD**-0.5

    c_bias.wait()
    c_len.wait()
    c_gate = load(17, gate_h.at[0], gate)
    c_up = load(18, up_h.at[0], up)
    c_down = load(19, down_h.at[0], down)

    position = iota((32, 1024), 1)
    for g in range(groups):
        blocks = []
        for h in range(4):
            half = queries[8 * g : 8 * g + 8, 128 * (h // 2) : 128 * (h // 2) + 128]
            turned = pltpu.roll(half, 64, 1)
            both = jnp.where(low, half, turned) if h % 2 == 0 else jnp.where(low, turned, half)
            blocks.append(jnp.concatenate([jnp.where(own[j], both, 0.0) for j in range(4)], axis=1))
        spread = jnp.concatenate(blocks, axis=0).astype(BF16)
        c_key[g].wait()
        raw = jnp.dot(spread, key[pl.ds(8 * g, 8)].reshape(512, 1024), preferred_element_type=F32)
        s = jnp.concatenate([raw[8 * h : 8 * h + 8] + bias[h] for h in range(4)], axis=0)
        length = jnp.zeros((8, 128), jnp.int32)
        for r in range(8):
            length = jnp.where(sub == r, lens[8 * g + r], length)
        length = jnp.concatenate([length] * 8, axis=1)
        length = jnp.concatenate([length] * 4, axis=0)
        inside = position < length
        fall = jnp.where(inside, jnp.minimum(-s, 0.0) - jnp.log(1.0 + jnp.exp(-jnp.abs(s))), 0.0)
        scores[pl.ds(32 * g, 32), :] = jnp.where(inside, s, -jnp.inf)
        pieces = [fall[:, 256 * b : 256 * b + 256] for b in range(4)]
        later = [None] * 4
        later[3] = jnp.zeros_like(pieces[3])
        for b in (2, 1, 0):
            later[b] = later[b + 1] + pieces[b + 1]
        for b in range(4):
            stacked = jnp.concatenate([pieces[b], later[b]], axis=1)
            high = stacked.astype(BF16)
            at = 128 * g + 32 * b
            falls_ref[pl.ds(at, 32), :] = high
            falls_ref[pl.ds(128 * groups + at, 32), :] = (stacked - high.astype(F32)).astype(BF16)

    total = jnp.dot(falls_ref[pl.ds(0, 128 * groups), :], tri[...], preferred_element_type=F32) + jnp.dot(
        falls_ref[pl.ds(128 * groups, 128 * groups), :], tri[...], preferred_element_type=F32
    )
    weights = []
    for g in range(groups):
        here = jnp.concatenate([total[128 * g + 32 * b : 128 * g + 32 * b + 32] for b in range(4)], axis=1)
        weights.append(jnp.exp(scores[pl.ds(32 * g, 32), :] + here).astype(BF16))
    for g in range(groups):
        c_val[g].wait()
    attended = []
    for g in range(groups):
        mixed = lax.dot_general(
            weights[g], val[pl.ds(8 * g, 8)].reshape(512, 1024), (((1,), (1,)), ((), ())), preferred_element_type=F32
        )
        heads = []
        for h in range(4):
            m = [jnp.where(own[j], mixed[8 * h : 8 * h + 8, 128 * j : 128 * j + 128], 0.0) for j in range(4)]
            m = (m[0] + m[1]) + (m[2] + m[3])
            heads.append(m + pltpu.roll(m, 64, 1))
        attended.append(jnp.concatenate([jnp.where(low, heads[0], heads[1]), jnp.where(low, heads[2], heads[3])], axis=1))
    attended = jnp.concatenate(attended, axis=0).astype(BF16)
    c_wo.wait()
    part_out = jnp.dot(attended, wo[...], preferred_element_type=F32).astype(BF16)
    for h in range(2):
        part[h] = part_out[:, half_width * h : half_width * (h + 1)]

    pl.semaphore_wait(barrier, n_ep + n_tp - 2)

    def push(src, dst, n, device):
        pltpu.make_async_remote_copy(
            src_ref=src, dst_ref=dst, send_sem=send_sem.at[n], recv_sem=recv_sem.at[n],
            device_id=device, device_id_type=MESH,
        ).start()

    def landed(some, n, sems):
        pltpu.make_async_copy(some, some, sems.at[n]).wait()

    for i in range(1, n_tp):
        t = lax.rem(tp + i, n_tp)
        push(part.at[lax.rem(t, 2)], part_in.at[tp], PARTS, (ep, t))
    part_in[tp] = part[core]

    c_routes.wait()
    c_rw.wait()
    c_fgain.wait()
    place = iota((2 * n_ep, seqs), 0)
    expert = place - jnp.where(place >= n_ep, n_ep, 0)
    slot = jnp.where(place >= n_ep, 1.0, 0.0)
    first = jnp.where(routes[0:1, :] == expert, 1.0, 0.0)
    second = jnp.where(routes[1:2, :] == expert, 1.0, 0.0)
    chosen = first + second
    above = jnp.where(iota((seqs, seqs), 0) < iota((seqs, seqs), 1), 1.0, 0.0)
    before = jnp.dot(chosen.astype(BF16), above.astype(BF16), preferred_element_type=F32)
    here = jnp.where(before == slot, 1.0, 0.0)
    plan = (chosen * here).astype(BF16)
    gather = jnp.transpose((first * rw[0:1, :] + second * rw[1:2, :]) * here)
    gather_high = gather.astype(BF16)
    gather_rest = (gather - gather_high.astype(F32)).astype(BF16)
    turned = (((1,), (1,)), ((), ()))
    c_wk.wait()
    nk_o[...] = lax.dot_general(normed, wk[...], turned, preferred_element_type=F32).astype(BF16)
    c_wv.wait()
    nv_o[...] = lax.dot_general(normed, wv[...], turned, preferred_element_type=F32).astype(BF16)

    landed(part_in.at[pl.ds(0, n_tp - 1)], PARTS, recv_sem)
    summed = part_in[0].astype(F32)
    for t in range(1, n_tp):
        summed = summed + part_in[t].astype(F32)
    token_half = jnp.where(core == 0, tokens[:, :half_width], tokens[:, half_width:])
    residual = (token_half + summed).astype(BF16)

    def store_rows(j, both):
        for s in range(2):
            wide[pl.ds(4 * s + j, n_ep, stride=8), :] = both[n_ep * s : n_ep * (s + 1)]

    def read_rows(j):
        return jnp.concatenate([wide[pl.ds(4 * s + j, n_ep, stride=8), :] for s in range(2)], axis=0)

    for j in range(4):
        store_rows(j, jnp.dot(plan, residual[:, 128 * j : 128 * j + 128], preferred_element_type=F32))
    disp[...] = wide[...].astype(BF16).reshape(n_ep, 8, 128)
    for k, p in enumerate(targets):
        push(disp.at[p], disp_in.at[k], FAR if k < far else NEAR, (p, tp))
    disp_in[n_ep - 1] = disp[ep]
    res_mine[...] = residual
    push(res_mine, res_other, RESIDUAL, (ep, partner))

    far_slots, near_slots = pl.ds(0, far), pl.ds(far, far)
    landed(disp_in.at[pl.ds(far, far - 1)], NEAR, recv_sem)
    push(disp_in.at[near_slots], disp_other.at[near_slots], PAIR_NEAR, (ep, partner))
    c_gate.wait()
    c_up.wait()
    c_down.wait()
    landed(disp_in.at[far_slots], FAR, recv_sem)
    push(disp_in.at[far_slots], disp_other.at[far_slots], PAIR_FAR, (ep, partner))

    def columns(h, j, size):
        return pl.ds(pl.multiple_of(half_width * h + size * j, size), size)

    squares = jnp.zeros((2 * n_ep, 128), F32)
    for h, block in ((core, disp_in), (1 - core, disp_other)):
        if block is disp_other:
            landed(disp_other.at[near_slots], PAIR_NEAR, recv_sem)
            landed(disp_other.at[far_slots], PAIR_FAR, recv_sem)
        wide[...] = block[...].astype(F32).reshape(n_ep * 8, 128)
        for j in range(4):
            values = read_rows(j)
            squares = squares + values * values
            plain[:, columns(h, j, 128)] = values
    factor = lax.rsqrt(jnp.sum(squares, axis=-1, keepdims=True) / width + EPS)
    rows[...] = (plain[...] * factor * fgain[...]).astype(BF16)

    units = gate.shape[1]
    for c in range(0, units, 256):
        size = min(256, units - c)
        a = jnp.dot(rows[...], gate[:, c : c + size], preferred_element_type=F32)
        b = jnp.dot(rows[...], up[:, c : c + size], preferred_element_type=F32)
        hidden[:, c : c + size] = (a / (1.0 + jnp.exp(-a)) * b).astype(BF16)

    def lower(h, j):
        return jnp.dot(hidden[...], down[:, columns(h, j, 256)], preferred_element_type=F32)

    for j in range(2):
        pair_out[j] = lower(1 - core, j).astype(BF16)
        push(pair_out.at[j], pair_in.at[j], PAIR_BACK, (ep, partner))
    mine = [lower(core, j) for j in range(2)]
    landed(pair_in, PAIR_BACK, recv_sem)
    for j in range(2):
        out = mine[j] + pair_in[j].astype(F32)
        for i in range(2):
            store_rows(2 * j + i, out[:, 128 * i : 128 * i + 128])
    back[...] = wide[...].astype(BF16).reshape(n_ep, 8, 128)
    for k, p in enumerate(sources):
        push(back.at[k], back_in.at[ep], BACK, (p, tp))
    back_in[ep] = back[n_ep - 1]

    landed(back_in.at[pl.ds(0, n_ep - 1)], BACK, recv_sem)
    wide[...] = back_in[...].astype(F32).reshape(n_ep * 8, 128)
    picked = jnp.concatenate([read_rows(j) for j in range(4)], axis=1).astype(BF16)
    fin[...] = (
        jnp.dot(gather_high, picked, preferred_element_type=F32)
        + jnp.dot(gather_rest, picked, preferred_element_type=F32)
    ).astype(BF16)
    for i in range(1, n_tp):
        push(fin, fin_in.at[tp], LAST, (ep, lax.rem(tp + i, n_tp)))
    fin_in[tp] = fin[...]

    landed(res_other, RESIDUAL, recv_sem)
    landed(part_in.at[pl.ds(0, n_tp - 1)], PARTS, send_sem)
    landed(res_mine, RESIDUAL, send_sem)
    landed(disp.at[far_slots], FAR, send_sem)
    landed(disp.at[pl.ds(0, far - 1)], NEAR, send_sem)
    landed(disp_in.at[near_slots], PAIR_NEAR, send_sem)
    landed(disp_in.at[far_slots], PAIR_FAR, send_sem)
    landed(pair_out, PAIR_BACK, send_sem)
    landed(back.at[pl.ds(0, n_ep - 1)], BACK, send_sem)
    landed(fin_in.at[pl.ds(0, n_tp - 1)], LAST, recv_sem)
    for h in range(2):
        kept = jnp.where(core == h, res_mine[...].astype(F32), res_other[...].astype(F32))
        moved = fin_in[h].astype(F32)
        for t in range(2 + h, n_tp, 2):
            moved = moved + fin_in[t].astype(F32)
        mixed_o[:, half_width * h : half_width * (h + 1)] = (kept + moved).astype(BF16)
    landed(fin_in.at[pl.ds(0, n_tp - 1)], LAST, send_sem)


def write_out(*refs):
    ins, outs, sems = refs[:3], refs[3:6], refs[6]
    copies = [pltpu.make_async_copy(ins[i], outs[i], sems.at[i]) for i in range(3)]
    for copy in copies:
        copy.start()
    for copy in copies:
        copy.wait()


def solution(mesh):
    n_ep, n_tp = mesh.shape["ep"], mesh.shape["tp"]

    def body(*args):
        (tokens, attn_gain, w_query, w_key, w_value, attn_bias, key_cache, value_cache, lengths, w_out,
         ffn_gain, routes, route_weight, expert_gate, expert_up, expert_down) = args
        seqs, width = tokens.shape
        units = expert_gate.shape[2]
        half = width // 2
        operands = (
            tokens, attn_gain.reshape(1, width), w_query, w_key.T, w_value.T, attn_bias, key_cache, value_cache, lengths,
            w_out, ffn_gain.reshape(1, width), routes.T, route_weight.T, expert_gate, expert_up, expert_down,
        )
        vmem, smem = pltpu.VMEM, pltpu.SMEM

        def run(*refs):
            kernel(n_ep, n_tp, *refs)

        results = pl.pallas_call(
            run,
            name="layer",
            out_shape=(
                jax.ShapeDtypeStruct(tokens.shape, BF16),
                jax.ShapeDtypeStruct((seqs, w_key.shape[1]), BF16),
                jax.ShapeDtypeStruct((seqs, w_value.shape[1]), BF16),
            ),
            in_specs=[pl.BlockSpec(memory_space=pltpu.HBM)] * len(operands),
            out_specs=(pl.BlockSpec(memory_space=vmem),) * 3,
            scratch_shapes=[
                vmem(tokens.shape, BF16), vmem((1, width), F32), vmem(w_query.shape, BF16), vmem(w_key.shape[::-1], BF16),
                vmem(w_value.shape[::-1], BF16), smem(attn_bias.shape, F32), vmem(key_cache.shape, BF16),
                vmem(value_cache.shape, BF16), smem(lengths.shape, jnp.int32), vmem(w_out.shape, BF16),
                vmem((1, width), F32), vmem(routes.shape[::-1], jnp.int32), vmem(route_weight.shape[::-1], F32),
                vmem(expert_gate.shape[1:], BF16), vmem(expert_up.shape[1:], BF16), vmem(expert_down.shape[1:], BF16),
                vmem((512, 256), BF16), vmem((4 * seqs, 1024), F32), vmem((32 * seqs, 512), BF16), vmem((2, seqs, half), BF16),
                vmem((n_tp, seqs, half), BF16), *[vmem((n_ep, 8, 128), BF16)] * 5,
                *[vmem((2, 2 * n_ep, half // 2), BF16)] * 2, vmem((seqs, half), BF16),
                vmem((n_tp, seqs, half), BF16), *[vmem((seqs, half), BF16)] * 2, vmem((n_ep * 8, 128), F32),
                vmem((2 * n_ep, width), F32), vmem((2 * n_ep, width), BF16), vmem((2 * n_ep, units), BF16),
                pltpu.SemaphoreType.DMA((20,)), pltpu.SemaphoreType.DMA((9,)), pltpu.SemaphoreType.DMA((9,)),
            ],
            compiler_params=pltpu.CompilerParams(
                collective_id=0, has_side_effects=True, vmem_limit_bytes=48 * 1024 * 1024
            ),
        )(*[pltpu.with_memory_space_constraint(x, pltpu.HBM) for x in operands])

        return pl.pallas_call(
            write_out,
            name="write_out",
            out_shape=tuple(pltpu.HBM(r.shape, r.dtype) for r in results),
            in_specs=[pl.BlockSpec(memory_space=vmem)] * 3,
            out_specs=(pl.BlockSpec(memory_space=pltpu.HBM),) * 3,
            scratch_shapes=[pltpu.SemaphoreType.DMA((3,))],
            compiler_params=pltpu.CompilerParams(vmem_limit_bytes=1024 * 1024),
        )(*[pltpu.with_memory_space_constraint(r, vmem) for r in results])

    return jax.shard_map(
        body,
        mesh=mesh,
        in_specs=(
            P("ep", None), P(), P(None, "tp"), P(None, "tp"), P(None, "tp"), P("tp"), P("ep", "tp", None),
            P("ep", "tp", None), P("ep"), P("tp", None), P(), P("ep", None), P("ep", None), P("ep", None, "tp"),
            P("ep", None, "tp"), P("ep", "tp", None),
        ),
        out_specs=(P("ep", None), P("ep", "tp"), P("ep", "tp")),
        check_vma=False,
    )
```

time: 41.3 us -> 38.9 us (0.942)
  Pallas kernels: 40.6 us -> 38.1 us
    pallas_call x1, Pallas kernels: 39.9 us -> 37.5 us  [body(): pl.pallas_call(run, name='layer', out_shape=(jax.ShapeDtypeStruct(tokens....]
where the time goes in v3:
time: 38.9 us; the launch traced here: 38.8 us
  Pallas kernels  38.1 us (98%)
  between operations  0.65 us (2%)
    pallas_call x1, Pallas kernels, body(): pl.pallas_call(run, name='layer', out_shape=(jax.ShapeDtypeStruct(tokens....  37.5 us

profile of v3, /device:TPU:1, one launch (start us, length us, event | category | flops | bytes accessed | tf_op | source)
XLA Modules:
  0.0 38.8 jit_solution(6939953649971646068)
XLA Ops:
  0.6 37.5 %layer.1 = (bf16[24,1024]{1,0:T(8,128)(2,1)S(1)}, bf16[24,64]{1,0:T(8,128)(2,1)S(1)}, bf16[24,64]{1,0:T(8,128)(2,1)S(1)}) custom-call(bf16[24,1024]{1,0:T(8,128)(2,1)} %refs_0_.1, f32[1,1024]{1,0:T(1,128)} %bitcast.8, bf16[1024,256]{1,0:T(8,128)(2,1)} %refs_2_.1, bf16[64,1024]{1,0:T(8,128)(2,1)} %bitcast.6, bf16[64,1024]{1,0:T(8,128)(2,1)} %bitcast.7, ...), custom_call_target="tpu_custom_call" | custom-call | tf_op jit(solution)/shard_map/layer/pallas_call | solution.py:327
  38.1 0.7 %write_out.1 = (bf16[24,1024]{1,0:T(8,128)(2,1)}, bf16[24,64]{1,0:T(8,128)(2,1)}, bf16[24,64]{1,0:T(8,128)(2,1)}) custom-call(bf16[24,1024]{1,0:T(8,128)(2,1)S(1)} %get-tuple-element.6.refs_0_, bf16[24,64]{1,0:T(8,128)(2,1)S(1)} %get-tuple-element.7.refs_1_, bf16[24,64]{1,0:T(8,128)(2,1)S(1)} %get-tuple-element.8.refs_2_), custom_call_target="tpu_custom_call" | custom-call | tf_op jit(solution)/shard_map/write_out/pallas_call | solution.py:355
